TPU v7x, 32 devices: a whole 2x2x4 slice. The times are simulated.
32 devices in a mesh: ep: 4 (over y, x), tp: 8 (over z, core).
Axes of the slice: x: 2, y: 2, z: 4, core: 2. Of those that a mesh axis runs over, the one named last changes fastest.
Arguments:
- residual: bfloat16 [128, 2048], P('ep'), may hold values from -20 to 20
- cache_latent: bfloat16 [128, 2048, 256], P(('ep', 'tp')), may hold values from -12 to 12
- cache_rope: bfloat16 [128, 32, 2048], P(('ep', 'tp')), may hold values from -6 to 6
- lengths: int32 [128], P(('ep', 'tp')), may hold values from 2 to 2048, as said below
- query_latent: bfloat16 [128, 32, 256], P(('ep', 'tp')), may hold values from -250 to 250
- query_rope: bfloat16 [128, 32, 32], P(('ep', 'tp')), may hold values from -6 to 6
- norm_gain: bfloat16 [2048], replicated, may hold values from 0.099609375 to 1.8984375
- latent_weight: bfloat16 [2048, 256], replicated, may hold values from -0.125 to 0.125
- latent_gain: bfloat16 [256], replicated, may hold values from 0.099609375 to 1.8984375
- rope_weight: bfloat16 [32, 2048], replicated, may hold values from -0.125 to 0.125
- value_weight: bfloat16 [256, 2048], replicated, may hold values from -0.375 to 0.375
- out_weight: bfloat16 [2048, 2048], P('tp'), may hold values from -1 to 1
- mixer_gain: bfloat16 [2048], replicated, may hold values from 0.099609375 to 1.8984375
- group_router: bfloat16 [2048, 4], replicated, may hold values from -0.0625 to 0.0625
- expert_router: bfloat16 [2048, 8], replicated, may hold values from -0.0625 to 0.0625
- expert_ids: int32 [128, 2], P('ep'), may hold values from 0 to 7, as said below
- gate_weight: bfloat16 [8, 2048, 4096], P('ep', None, 'tp'), may hold values from -0.125 to 0.125
- up_weight: bfloat16 [8, 2048, 4096], P('ep', None, 'tp'), may hold values from -0.125 to 0.125
- down_weight: bfloat16 [8, 4096, 2048], P('ep', 'tp'), may hold values from -0.75 to 0.75
Outputs:
- mixed: bfloat16 [128, 2048], P('ep')
- new_latent: bfloat16 [128, 256], P(('ep', 'tp'))
- new_rope_key: bfloat16 [128, 32], P(('ep', 'tp'))
Inputs may be any that keep to these rules, and one draw needn't show every extreme that they name: `lengths`: every sequence has 2 or more cached positions, and in every draw some sequence has all 2048. `expert_ids`: each row names 2 different experts of one group; group g holds experts g * 2 to g * 2 + 1. Among the rows of one index of ep (aligned blocks of 32 rows) no expert is named more than 16 times, and in every draw some expert is named exactly 16 times in every block.
All inputs are finite; a program needn't handle non-finite values.
Results may differ from a plain program's by a relative error of at most 0.012.
Values may be sent and summed in bfloat16 or wider, within the bound.
A program may use at most 64 MiB of HBM per device.

v0:
```python
import jax
import jax.numpy as jnp
from jax import lax
from jax.sharding import PartitionSpec as P

H = 32
KV = 256
ROPE = 32
NOPE = 64
V = 64
GROUPS = 4
TOPK = 2
NORM_EPSILON = 1e-06
ROPE_BASE = 10000.0


def inverse_rms(values):
    return lax.rsqrt(jnp.mean(values * values, axis=-1, keepdims=True) + NORM_EPSILON)


def rotate(vector, position):
    half_width = vector.shape[-1] // 2
    frequency = ROPE_BASE ** (
        -jnp.arange(0, vector.shape[-1], 2, dtype=jnp.float32) / vector.shape[-1]
    )
    angles = position[..., None] * frequency
    lower_half = vector[..., :half_width]
    upper_half = vector[..., half_width:]
    return jnp.concatenate(
        [
            lower_half * jnp.cos(angles) - upper_half * jnp.sin(angles),
            upper_half * jnp.cos(angles) + lower_half * jnp.sin(angles),
        ],
        axis=-1,
    )


def dispatch_table(expert_rows, experts, capacity):
    flat_ids = expert_rows.reshape(-1)
    hit_table = (flat_ids[:, None] == jnp.arange(experts, dtype=jnp.int32)[None, :]).astype(
        jnp.int32
    )
    slot_rank = jnp.sum((jnp.cumsum(hit_table, axis=0) - hit_table) * hit_table, axis=1)
    slot_index = flat_ids * capacity + slot_rank
    picked = (
        slot_index[None, :] == jnp.arange(experts * capacity, dtype=jnp.int32)[:, None]
    ).astype(jnp.float32)
    return picked.reshape(experts * capacity, expert_rows.shape[0], expert_rows.shape[1])


def route_weights(expert_in, group_router, expert_router, expert_ids, per_group):
    group_logits = jnp.dot(expert_in, group_router, preferred_element_type=jnp.float32)
    expert_logits = jnp.dot(expert_in, expert_router, preferred_element_type=jnp.float32)
    chosen = expert_ids[:, 0] // per_group
    group_hit = (
        jnp.arange(group_logits.shape[1], dtype=jnp.int32)[None, :] == chosen[:, None]
    ).astype(jnp.float32)
    chosen_logit = jnp.sum(group_logits * group_hit, axis=1, keepdims=True)
    group_share = 1.0 / jnp.sum(jnp.exp(group_logits - chosen_logit), axis=1)
    expert_hit = (
        expert_ids[:, :, None] == jnp.arange(expert_logits.shape[1], dtype=jnp.int32)[None, None, :]
    ).astype(jnp.float32)
    picked_logit = jnp.sum(expert_hit * expert_logits[:, None, :], axis=2)
    inner_share = 1.0 / jnp.sum(
        jnp.exp(picked_logit[:, None, :] - picked_logit[:, :, None]), axis=2
    )
    return group_share[:, None] * inner_share


def on_device(
    residual,
    cache_latent,
    cache_rope,
    lengths,
    query_latent,
    query_rope,
    norm_gain,
    latent_weight,
    latent_gain,
    rope_weight,
    value_weight,
    out_weight,
    mixer_gain,
    group_router,
    expert_router,
    expert_ids,
    gate_weight,
    up_weight,
    down_weight,
):
    ep_count = lax.axis_size("ep")
    seq_count = cache_latent.shape[0]
    group_rows = residual.shape[0]
    model_width = residual.shape[1]
    resid_f = residual.astype(jnp.float32)
    own_rows = lax.dynamic_slice_in_dim(resid_f, lax.axis_index("tp") * seq_count, seq_count, 0)
    normed = (own_rows * inverse_rms(own_rows) * norm_gain.astype(jnp.float32)).astype(jnp.bfloat16)
    latent_raw = jnp.dot(normed, latent_weight, preferred_element_type=jnp.float32)
    new_latent = (latent_raw * inverse_rms(latent_raw) * latent_gain.astype(jnp.float32)).astype(
        jnp.bfloat16
    )
    positions = lengths.astype(jnp.float32)
    rope_raw = jnp.dot(normed, rope_weight.T, preferred_element_type=jnp.float32)
    new_rope_key = rotate(rope_raw, positions).astype(jnp.bfloat16)
    query_turned = rotate(query_rope.astype(jnp.float32), positions[:, None]).astype(jnp.bfloat16)
    score_scale = (NOPE + ROPE) ** (-0.5)
    cached = (
        jnp.einsum("shc,spc->shp", query_latent, cache_latent, preferred_element_type=jnp.float32)
        + jnp.einsum("shr,srp->shp", query_turned, cache_rope, preferred_element_type=jnp.float32)
    ) * score_scale
    keeping = (
        jnp.arange(cache_latent.shape[1], dtype=jnp.int32)[None, None, :] < lengths[:, None, None]
    )
    cached = jnp.where(keeping, cached, -jnp.inf)
    fresh = (
        jnp.einsum("shc,sc->sh", query_latent, new_latent, preferred_element_type=jnp.float32)
        + jnp.einsum("shr,sr->sh", query_turned, new_rope_key, preferred_element_type=jnp.float32)
    ) * score_scale
    row_top = jnp.maximum(jnp.max(cached, axis=2), fresh)
    cached_exp = jnp.exp(cached - row_top[:, :, None])
    fresh_exp = jnp.exp(fresh - row_top)
    denominator = jnp.sum(cached_exp, axis=2) + fresh_exp
    cached_weight = (cached_exp / denominator[:, :, None]).astype(jnp.bfloat16)
    fresh_weight = (fresh_exp / denominator).astype(jnp.bfloat16)
    mixed_latent = (
        jnp.einsum("shp,spc->shc", cached_weight, cache_latent, preferred_element_type=jnp.float32)
        + fresh_weight.astype(jnp.float32)[:, :, None] * new_latent.astype(jnp.float32)[:, None, :]
    ).astype(jnp.bfloat16)
    head_values = jnp.einsum(
        "shc,chv->shv",
        mixed_latent,
        value_weight.reshape(KV, H, V),
        preferred_element_type=jnp.float32,
    ).astype(jnp.bfloat16)
    by_heads = lax.all_to_all(head_values, "tp", split_axis=1, concat_axis=0, tiled=True)
    head_terms = jnp.dot(
        by_heads.reshape(group_rows, -1), out_weight, preferred_element_type=jnp.float32
    )
    attended = lax.psum(head_terms, "tp")
    after_attention = (resid_f + attended).astype(jnp.bfloat16)
    after_f = after_attention.astype(jnp.float32)
    expert_in = (after_f * inverse_rms(after_f) * mixer_gain.astype(jnp.float32)).astype(
        jnp.bfloat16
    )
    experts = expert_router.shape[1]
    capacity = 2 * group_rows * TOPK // experts
    route_weight = route_weights(
        expert_in, group_router, expert_router, expert_ids, experts // GROUPS
    )
    picked = dispatch_table(expert_ids, experts, capacity)
    select_rows = jnp.sum(picked, axis=2).astype(jnp.bfloat16)
    outbound = jnp.dot(select_rows, expert_in, preferred_element_type=jnp.float32).astype(
        jnp.bfloat16
    )
    outbound = outbound.reshape(ep_count, gate_weight.shape[0], capacity, model_width)
    rows = lax.all_to_all(outbound, "ep", split_axis=0, concat_axis=0, tiled=True)
    gate_value = jnp.einsum("secd,edf->secf", rows, gate_weight, preferred_element_type=jnp.float32)
    up_value = jnp.einsum("secd,edf->secf", rows, up_weight, preferred_element_type=jnp.float32)
    activation = (jax.nn.silu(gate_value) * up_value).astype(jnp.bfloat16)
    expert_terms = jnp.einsum(
        "secf,efd->secd", activation, down_weight, preferred_element_type=jnp.float32
    )
    combine = jnp.sum(picked * route_weight[None, :, :], axis=2).T
    summed_terms = lax.psum_scatter(expert_terms, "tp", scatter_dimension=3, tiled=True)
    returned_terms = lax.all_to_all(summed_terms, "ep", split_axis=0, concat_axis=0, tiled=True)
    share_width = returned_terms.shape[3]
    moe_part = jnp.dot(
        combine, returned_terms.reshape(-1, share_width), precision=lax.Precision.HIGHEST
    )
    after_cols = lax.dynamic_slice_in_dim(
        after_f, lax.axis_index("tp") * share_width, share_width, 1
    )
    mixed_share = (after_cols + moe_part).astype(jnp.bfloat16)
    mixed = lax.all_gather(mixed_share, "tp", axis=1, tiled=True)
    return (mixed, new_latent, new_rope_key)


def solution(mesh):
    in_specs = (
        P("ep", None),
        P(("ep", "tp"), None, None),
        P(("ep", "tp"), None, None),
        P(("ep", "tp")),
        P(("ep", "tp"), None, None),
        P(("ep", "tp"), None, None),
        P(),
        P(),
        P(),
        P(),
        P(),
        P("tp", None),
        P(),
        P(),
        P(),
        P("ep", None),
        P("ep", None, "tp"),
        P("ep", None, "tp"),
        P("ep", "tp", None),
    )
    out_specs = (P("ep", None), P(("ep", "tp"), None), P(("ep", "tp"), None))
    return jax.shard_map(
        on_device, mesh=mesh, in_specs=in_specs, out_specs=out_specs, check_vma=False
    )
```

profile of v0, /device:TPU:0, one launch (start us, length us, event | category | flops | bytes accessed | tf_op | source)
XLA Modules:
  0.0 177.1 jit_solution(6395437696958432695)
XLA Ops:
  7.2 0.8 convert_element_type.79
  8.0 0.7 iota_compare_fusion.2
  8.7 0.9 convert_element_type.77
  9.8 0.7 convert_element_type.80
  10.5 0.8 convert_element_type.78
  11.3 1.1 fusion.50
  12.4 1.6 multiply_reduce_fusion.2
  14.7 3.5 %fusion.58 = f32[4,32,2048]{2,1,0:T(8,128)S(1)} fusion(bf16[4,32,256]{2,1,0:T(8,128)(2,1)} %param.23, bf16[4,2048,256]{2,1,0:T(8,128)(2,1)} %param.20), kind=kOutput, calls=%fused_computation.90 | convolution fusion | flops 134217728 | bytes 5308416 | tf_op jit(solution)/shard_map/shc,spc->shp/dot_general | solution.py:108
  19.8 1.5 copy.61
  21.3 3.1 %fusion.23 = bf16[4,32,256]{2,1,0:T(8,128)(2,1)S(1)} fusion(bf16[4,2048,256]{2,1,0:T(8,128)(2,1)} %param.20, f32[4,32,2048]{2,1,0:T(8,128)S(1)} %get-tuple-element.18, f32[4,32]{1,0:T(4,128)S(1)} %get-tuple-element.12, f32[4,32]{1,0:T(4,128)S(1)} %fusion.44, f32[4,256]{1,0:T(4,128)S(1)} %get-tuple-element.7, f32[4,32]{1,0:T(4,128)S(1)} %get-tuple-element.11), kind=kOutput, calls=%fused_computation.16 | convolution fusion | flops 135102464 | bytes 5314048 | tf_op jit(solution)/shard_map/shp,spc->shc/dot_general | solution.py:126
  24.8 0.7 reshape.194
  25.5 6.4 %all-to-all-start = ((bf16[8,2,512]{2,1,0:T(2,128)(2,1)}), bf16[8,2,512]{2,1,0:T(2,128)(2,1)S(1)}, u32[]{:S(2)}, u32[]{:S(2)}) async-start(bf16[8,2,512]{2,1,0:T(2,128)(2,1)} %reshape.194), calls=%async_computation | async-start | bytes 32768 | tf_op jit(solution)/shard_map/all_to_all | solution.py:135
  32.7 4.8 %all-to-all-done = bf16[8,2,512]{2,1,0:T(2,128)(2,1)S(1)} async-done(((bf16[8,2,512]{2,1,0:T(2,128)(2,1)}), bf16[8,2,512]{2,1,0:T(2,128)(2,1)S(1)}, u32[]{:S(2)}, u32[]{:S(2)}) %all-to-all-start) | async-done | bytes 16416 | tf_op jit(solution)/shard_map/all_to_all | solution.py:135
  37.7 1.0 fusion.59
  38.8 53.8 %all-reduce.2.cloned.1.call-done = f32[32,2048]{1,0:T(8,128)} async-done(((f32[32,2048]{1,0:T(8,128)}), f32[32,2048]{1,0:T(8,128)}) %all-reduce.2.cloned.1.call-update) | async-done | bytes 262160 | tf_op jit(solution)/shard_map/psum | solution.py:139
  92.6 1.1 multiply_reduce_fusion
  94.6 10.6 %all_to_all.25 = bf16[4,2,16,2048]{3,2,1,0:T(8,128)(2,1)S(1)} all-to-all(bf16[4,2,16,2048]{3,2,1,0:T(8,128)(2,1)S(1)} %bitcast.81), channel_id=1, replica_groups=mesh['ep'=4,'tp'=8] {'ep'}, dimensions={0} | all-to-all | bytes 1048576 | tf_op jit(solution)/shard_map/all_to_all | solution.py:156
  105.2 3.0 %fusion.11 = f32[4,2,16,512]{3,2,0,1:T(8,128)S(1)} fusion(bf16[2,2048,512]{2,1,0:T(8,128)(2,1)} %param.35, bf16[4,2,16,2048]{3,2,1,0:T(8,128)(2,1)S(1)} %all_to_all.25), kind=kOutput, calls=%fused_computation.11 | convolution fusion | flops 268435456 | bytes 4980736 | tf_op jit(solution)/shard_map/secd,edf->secf/dot_general | solution.py:157
  108.2 6.0 %fusion.6 = f32[4,2,16,2048]{3,2,0,1:T(8,128)} fusion(bf16[2,512,2048]{2,1,0:T(8,128)(2,1)} %param.37, bf16[2,2048,512]{2,1,0:T(8,128)(2,1)} %param.36, bf16[4,2,16,2048]{3,2,1,0:T(8,128)(2,1)S(1)} %all_to_all.25, f32[4,2,16,512]{3,2,0,1:T(8,128)S(1)} %fusion.11), kind=kOutput, calls=%fused_computation.6 | convolution fusion | flops 537264128 | bytes 10223616 | tf_op jit(solution)/shard_map/secf,efd->secd/dot_general | solution.py:160
  114.3 30.9 %reduce-scatter.2.cloned.1.call-done = f32[4,2,16,256]{3,2,0,1:T(8,128)} async-done(((f32[4,2,16,2048]{3,2,0,1:T(8,128)}), f32[4,2,16,256]{3,2,0,1:T(8,128)}) %reduce-scatter.2.cloned.1.call-update) | async-done | bytes 131088 | tf_op jit(solution)/shard_map/reduce_scatter | solution.py:164
  145.2 1.6 copy.68
  146.8 3.7 %all-to-all-start.2 = ((f32[4,2,16,256]{3,2,1,0:T(8,128)}), f32[4,2,16,256]{3,2,1,0:T(8,128)S(1)}, u32[]{:S(2)}, u32[]{:S(2)}) async-start(f32[4,2,16,256]{3,2,1,0:T(8,128)} %copy.68), calls=%async_computation.3 | async-start | bytes 262144 | tf_op jit(solution)/shard_map/all_to_all | solution.py:165
  151.1 4.4 %all-to-all-done.2 = f32[4,2,16,256]{3,2,1,0:T(8,128)S(1)} async-done(((f32[4,2,16,256]{3,2,1,0:T(8,128)}), f32[4,2,16,256]{3,2,1,0:T(8,128)S(1)}, u32[]{:S(2)}, u32[]{:S(2)}) %all-to-all-start.2) | async-done | bytes 131104 | tf_op jit(solution)/shard_map/all_to_all | solution.py:165
  155.6 14.0 %all_gather.3 = bf16[32,2048]{1,0:T(8,128)(2,1)S(1)} all-gather(bf16[32,256]{1,0:T(8,128)(2,1)S(1)} %fusion.25), channel_id=1, replica_groups=mesh['ep'=4,'tp'=8] {'tp'}, dimensions={1}, use_global_device_ids=true | all-gather | bytes 147456 | tf_op jit(solution)/shard_map/all_gather | solution.py:174
  (65 shorter events, 6.2 us)
Async XLA Ops:
  7.2 30.6 %copy-start = (bf16[256,2048]{1,0:T(8,128)(2,1)S(1)}, bf16[256,2048]{1,0:T(8,128)(2,1)}, u32[]{:S(2)}) copy-start(bf16[256,2048]{1,0:T(8,128)(2,1)} %param.30) | copy-start | bytes 3145732
  7.2 11.1 %copy-start.3 = (bf16[4,32,256]{2,1,0:T(8,128)(2,1)S(1)}, bf16[4,32,256]{2,1,0:T(8,128)(2,1)}, u32[]{:S(2)}) copy-start(bf16[4,32,256]{2,1,0:T(8,128)(2,1)} %param.23) | copy-start | bytes 196612
  7.2 11.7 %copy-start.2 = (bf16[4,32,2048]{2,1,0:T(8,128)(2,1)S(1)}, bf16[4,32,2048]{2,1,0:T(8,128)(2,1)}, u32[]{:S(2)}) copy-start(bf16[4,32,2048]{2,1,0:T(8,128)(2,1)} %param.21) | copy-start | bytes 1572868
  18.3 6.1 %copy-start.7 = (bf16[4,256]{1,0:T(4,128)(2,1)}, bf16[4,256]{1,0:T(4,128)(2,1)S(1)}, u32[]{:S(2)}) copy-start(bf16[4,256]{1,0:T(4,128)(2,1)S(1)} %get-tuple-element.27) | copy-start | bytes 6148
  21.2 10.7 %copy-start.5 = (s32[32,2]{0,1:T(2,128)S(1)}, s32[32,2]{0,1:T(2,128)}, u32[]{:S(2)}) copy-start(s32[32,2]{0,1:T(2,128)} %param.34) | copy-start | bytes 772
  21.3 11.4 %copy-start.6 = (bf16[2048]{0:T(1024)(128)(2,1)S(1)}, bf16[2048]{0:T(1024)(128)(2,1)}, u32[]{:S(2)}) copy-start(bf16[2048]{0:T(1024)(128)(2,1)} %param.31) | copy-start | bytes 12292
  21.3 71.3 %copy-start.1 = (bf16[32,2048]{1,0:T(8,128)(2,1)S(1)}, bf16[32,2048]{1,0:T(8,128)(2,1)}, u32[]{:S(2)}) copy-start(bf16[32,2048]{1,0:T(8,128)(2,1)} %param.19) | copy-start | bytes 393220
  21.3 72.5 %copy-start.8 = (bf16[2048,4]{0,1:T(4,128)(2,1)S(1)}, bf16[2048,4]{0,1:T(4,128)(2,1)}, u32[]{:S(2)}) copy-start(bf16[2048,4]{0,1:T(4,128)(2,1)} %param.32) | copy-start | bytes 49156
  21.3 72.7 %copy-start.4 = (bf16[2048,8]{0,1:T(8,128)(2,1)S(1)}, bf16[2048,8]{0,1:T(8,128)(2,1)}, u32[]{:S(2)}) copy-start(bf16[2048,8]{0,1:T(8,128)(2,1)} %param.33) | copy-start | bytes 98308
  25.5 12.0 %all-to-all-start = ((bf16[8,2,512]{2,1,0:T(2,128)(2,1)}), bf16[8,2,512]{2,1,0:T(2,128)(2,1)S(1)}, u32[]{:S(2)}, u32[]{:S(2)}) async-start(bf16[8,2,512]{2,1,0:T(2,128)(2,1)} %reshape.194), calls=%async_computation | async-start | bytes 32768 | tf_op jit(solution)/shard_map/all_to_all | solution.py:135
  31.9 60.7 %all-reduce.2.cloned.1.call-start = ((), (), s32[]{:S(2)}) async-start(), calls=%async_computation.4 | async-start | bytes 524288 | tf_op jit(solution)/shard_map/psum | solution.py:139
  38.7 106.5 %reduce-scatter.2.cloned.1.call-start = ((), (), s32[]{:S(2)}) async-start(), calls=%async_computation.5 | async-start | bytes 1179648 | tf_op jit(solution)/shard_map/reduce_scatter | solution.py:164
  146.8 8.7 %all-to-all-start.2 = ((f32[4,2,16,256]{3,2,1,0:T(8,128)}), f32[4,2,16,256]{3,2,1,0:T(8,128)S(1)}, u32[]{:S(2)}, u32[]{:S(2)}) async-start(f32[4,2,16,256]{3,2,1,0:T(8,128)} %copy.68), calls=%async_computation.3 | async-start | bytes 262144 | tf_op jit(solution)/shard_map/all_to_all | solution.py:165
Sparse Core Ops, SparseCore 0:
  38.9 53.6 all-reduce.1
  114.4 30.7 reduce-scatter.1
where the time goes:
time: 178 us; the launch traced here: 177 us
  waiting for transfers between devices  93.9 us (53%)
  blocking collectives  24.5 us (14%)
  matrix products  21.4 us (12%)
  between operations  14.3 us (8%)
  starting transfers between devices  10.1 us (6%)
  other arithmetic  7.81 us (4%)
  local copies, waits for them, and re-layouts  5.06 us (3%)
    psum x1, waiting for transfers between devices, on_device(): attended = lax.psum(head_terms, 'tp')  53.8 us
    reduce_scatter x1, waiting for transfers between devices, on_device(): lax.psum_scatter(expert_terms, 'tp', scatter_dimension=3, tiled=True)  30.9 us
    all_gather x1, blocking collectives, on_device(): mixed = lax.all_gather(mixed_share, 'tp', axis=1, tiled=True)  14 us
    all_to_all x1, blocking collectives, on_device(): lax.all_to_all(outbound, 'ep', split_axis=0, concat_axis=0, tiled=True)  10.6 us
    all_to_all x1, starting transfers between devices, on_device(): lax.all_to_all(head_values, 'tp', split_axis=1, concat_axis=0, tiled=True)  6.35 us
    dot_general x1, matrix products, on_device(): jnp.einsum('secf,efd->secd', activation, down_weight, preferred_element_t...  6.04 us
    all_to_all x1, waiting for transfers between devices, on_device(): lax.all_to_all(head_values, 'tp', split_axis=1, concat_axis=0, tiled=True)  4.83 us
    all_to_all x1, waiting for transfers between devices, on_device(): lax.all_to_all(summed_terms, 'ep', split_axis=0, concat_axis=0, tiled=True)  4.38 us
  transfers between devices with their start and end apart: 4, of which 4 were waited for; matrix products, arithmetic and copies ran while one was open for 1% of the time, Pallas kernels for 0%

commit v1 on v0

--- a/solution.py
+++ b/solution.py
@@ -136,7 +136,7 @@
     head_terms = jnp.dot(
         by_heads.reshape(group_rows, -1), out_weight, preferred_element_type=jnp.float32
     )
-    attended = lax.psum(head_terms, "tp")
+    attended = jnp.sum(lax.all_gather(head_terms, "tp"), axis=0)
     after_attention = (resid_f + attended).astype(jnp.bfloat16)
     after_f = after_attention.astype(jnp.float32)
     expert_in = (after_f * inverse_rms(after_f) * mixer_gain.astype(jnp.float32)).astype(

time: 178 us -> 153 us (0.86)
  waiting for transfers between devices: 93.9 us -> 61.8 us
  blocking collectives: 24.5 us -> 38.1 us
  starting transfers between devices: 10.1 us -> 3.69 us
    psum x1 -> x0, waiting for transfers between devices: 53.8 us -> none  [on_device(): attended = lax.psum(head_terms, 'tp')]
    all_gather x0 -> x1, waiting for transfers between devices: none -> 26.7 us  [on_device(): attended = jnp.sum(lax.all_gather(head_terms, 'tp'), axis=0)]
    all_to_all x0 -> x1, blocking collectives: none -> 11.8 us  [on_device(): lax.all_to_all(head_values, 'tp', split_axis=1, concat_axis=0, tiled=True)]
    all_to_all x1 -> x0, starting transfers between devices: 6.35 us -> none  [on_device(): lax.all_to_all(head_values, 'tp', split_axis=1, concat_axis=0, tiled=True)]
    all_to_all x1 -> x0, waiting for transfers between devices: 4.83 us -> none  [on_device(): lax.all_to_all(head_values, 'tp', split_axis=1, concat_axis=0, tiled=True)]
    all_to_all x1, blocking collectives: 10.6 us -> 12.4 us  [on_device(): lax.all_to_all(outbound, 'ep', split_axis=0, concat_axis=0, tiled=True)]
  transfers between devices with their start and end apart: 4 -> 3, of which waited for: 4 -> 3; matrix products, arithmetic and copies ran while one was open for 1% -> 1% of each run, Pallas kernels for 0% -> 0%
where the time goes in v1:
time: 153 us; the launch traced here: 152 us
  waiting for transfers between devices  61.8 us (40%)
  blocking collectives  38.1 us (25%)
  matrix products  21.3 us (14%)
  between operations  14.4 us (9%)
  other arithmetic  8.57 us (6%)
  local copies, waits for them, and re-layouts  4.45 us (3%)
  starting transfers between devices  3.69 us (2%)
    reduce_scatter x1, waiting for transfers between devices, on_device(): lax.psum_scatter(expert_terms, 'tp', scatter_dimension=3, tiled=True)  30.7 us
    all_gather x1, waiting for transfers between devices, on_device(): attended = jnp.sum(lax.all_gather(head_terms, 'tp'), axis=0)  26.7 us
    all_gather x1, blocking collectives, on_device(): mixed = lax.all_gather(mixed_share, 'tp', axis=1, tiled=True)  14 us
    all_to_all x1, blocking collectives, on_device(): lax.all_to_all(outbound, 'ep', split_axis=0, concat_axis=0, tiled=True)  12.4 us
    all_to_all x1, blocking collectives, on_device(): lax.all_to_all(head_values, 'tp', split_axis=1, concat_axis=0, tiled=True)  11.8 us
    dot_general x1, matrix products, on_device(): jnp.einsum('secf,efd->secd', activation, down_weight, preferred_element_t...  6.04 us
    all_to_all x1, waiting for transfers between devices, on_device(): lax.all_to_all(summed_terms, 'ep', split_axis=0, concat_axis=0, tiled=True)  4.38 us
    all_to_all x1, starting transfers between devices, on_device(): lax.all_to_all(summed_terms, 'ep', split_axis=0, concat_axis=0, tiled=True)  3.61 us
  transfers between devices with their start and end apart: 3, of which 3 were waited for; matrix products, arithmetic and copies ran while one was open for 1% of the time, Pallas kernels for 0%

profile of v1, /device:TPU:0, one launch (start us, length us, event | category | flops | bytes accessed | tf_op | source)
XLA Modules:
  0.0 152.4 jit_solution(17331043599545432066)
XLA Ops:
  7.3 0.8 convert_element_type.79
  8.0 0.7 iota_compare_fusion.2
  8.8 0.9 convert_element_type.77
  9.8 0.7 convert_element_type.80
  10.5 0.8 convert_element_type.78
  11.3 1.1 fusion.50
  12.4 1.6 %multiply_reduce_fusion.2 = (f32[4]{0:T(128)S(1)}, f32[4,256]{1,0:T(4,128)S(1)}) fusion(bf16[2048,256]{1,0:T(8,128)(2,1)} %param.26, f32[32,2048]{1,0:T(8,128)S(1)} %convert_element_type.77, s32[]{:T(128)S(6)} %select_n.17, f32[2048]{0:T(1024)S(1)} %convert_element_type.80, f32[4]{0:T(128)S(1)} %add_rsqrt_fusion.2), kind=kOutput, calls=%fused_computation.53 | convolution fusion | flops 4220924 | bytes 1094164 | tf_op jit(solution)/shard_map/dot_general | solution.py:98
  14.1 0.7 convert_element_type.82
  14.7 3.5 %fusion.58 = f32[4,32,2048]{2,1,0:T(8,128)S(1)} fusion(bf16[4,32,256]{2,1,0:T(8,128)(2,1)} %param.23, bf16[4,2048,256]{2,1,0:T(8,128)(2,1)} %param.20), kind=kOutput, calls=%fused_computation.90 | convolution fusion | flops 134217728 | bytes 5308416 | tf_op jit(solution)/shard_map/shc,spc->shp/dot_general | solution.py:108
  19.8 1.5 copy.61
  21.3 3.0 %fusion.23 = bf16[4,32,256]{2,1,0:T(8,128)(2,1)S(1)} fusion(bf16[4,2048,256]{2,1,0:T(8,128)(2,1)} %param.20, f32[4,32,2048]{2,1,0:T(8,128)S(1)} %get-tuple-element.18, f32[4,32]{1,0:T(4,128)S(1)} %get-tuple-element.12, f32[4,32]{1,0:T(4,128)S(1)} %fusion.44, f32[4,256]{1,0:T(4,128)S(1)} %get-tuple-element.7, f32[4,32]{1,0:T(4,128)S(1)} %get-tuple-element.11), kind=kOutput, calls=%fused_computation.16 | convolution fusion | flops 135102464 | bytes 5314048 | tf_op jit(solution)/shard_map/shp,spc->shc/dot_general | solution.py:126
  24.9 11.8 %all_to_all.25 = bf16[8,2,512]{2,1,0:T(2,128)(2,1)S(1)} all-to-all(bf16[8,2,512]{2,1,0:T(2,128)(2,1)S(1)} %reshape.195), channel_id=1, replica_groups=mesh['ep'=4,'tp'=8] {'tp'}, dimensions={0} | all-to-all | bytes 32768 | tf_op jit(solution)/shard_map/all_to_all | solution.py:135
  36.9 1.0 fusion.59
  38.8 26.7 %all-gather.3.cloned.1.call-done = f32[256,2048]{1,0:T(8,128)} async-done(((f32[32,2048]{1,0:T(8,128)}), f32[256,2048]{1,0:T(8,128)}) %all-gather.3.cloned.1.call-update) | async-done | bytes 2097168 | tf_op jit(solution)/shard_map/all_gather | solution.py:139
  65.5 1.7 %reduce_sum.113 = f32[32,2048]{1,0:T(8,128)S(1)} reduce(f32[8,32,2048]{2,1,0:T(8,128)} %bitcast.82, f32[]{:T(128)} %constant.56.clone.1), dimensions={0}, to_apply=%region_4.5 | reduce | flops 458752 | bytes 2359300 | tf_op jit(solution)/shard_map/reduce_sum | solution.py:139
  68.4 12.4 %all_to_all.26 = bf16[4,2,16,2048]{3,2,1,0:T(8,128)(2,1)S(1)} all-to-all(bf16[4,2,16,2048]{3,2,1,0:T(8,128)(2,1)S(1)} %bitcast.83), channel_id=1, replica_groups=mesh['ep'=4,'tp'=8] {'ep'}, dimensions={0} | all-to-all | bytes 1048576 | tf_op jit(solution)/shard_map/all_to_all | solution.py:156
  80.7 3.0 %fusion.11 = f32[4,2,16,512]{3,2,0,1:T(8,128)S(1)} fusion(bf16[2,2048,512]{2,1,0:T(8,128)(2,1)} %param.35, bf16[4,2,16,2048]{3,2,1,0:T(8,128)(2,1)S(1)} %all_to_all.26), kind=kOutput, calls=%fused_computation.11 | convolution fusion | flops 268435456 | bytes 4980736 | tf_op jit(solution)/shard_map/secd,edf->secf/dot_general | solution.py:157
  83.7 6.0 %fusion.6 = f32[4,2,16,2048]{3,2,0,1:T(8,128)} fusion(bf16[2,512,2048]{2,1,0:T(8,128)(2,1)} %param.37, bf16[2,2048,512]{2,1,0:T(8,128)(2,1)} %param.36, bf16[4,2,16,2048]{3,2,1,0:T(8,128)(2,1)S(1)} %all_to_all.26, f32[4,2,16,512]{3,2,0,1:T(8,128)S(1)} %fusion.11), kind=kOutput, calls=%fused_computation.6 | convolution fusion | flops 537264128 | bytes 10223616 | tf_op jit(solution)/shard_map/secf,efd->secd/dot_general | solution.py:160
  89.8 30.7 %reduce-scatter.2.cloned.1.call-done = f32[4,2,16,256]{3,2,0,1:T(8,128)} async-done(((f32[4,2,16,2048]{3,2,0,1:T(8,128)}), f32[4,2,16,256]{3,2,0,1:T(8,128)}) %reduce-scatter.2.cloned.1.call-update) | async-done | bytes 131088 | tf_op jit(solution)/shard_map/reduce_scatter | solution.py:164
  120.5 1.6 %copy.68 = f32[4,2,16,256]{3,2,1,0:T(8,128)} copy(f32[4,2,16,256]{3,2,0,1:T(8,128)} %reduce-scatter.2.cloned.1.call-done) | data formatting | bytes 262144 | tf_op jit(solution)/shard_map/reduce_scatter | solution.py:164
  122.1 3.6 %all-to-all-start.2 = ((f32[4,2,16,256]{3,2,1,0:T(8,128)}), f32[4,2,16,256]{3,2,1,0:T(8,128)S(1)}, u32[]{:S(2)}, u32[]{:S(2)}) async-start(f32[4,2,16,256]{3,2,1,0:T(8,128)} %copy.68), calls=%async_computation.3 | async-start | bytes 262144 | tf_op jit(solution)/shard_map/all_to_all | solution.py:165
  126.3 4.4 %all-to-all-done.2 = f32[4,2,16,256]{3,2,1,0:T(8,128)S(1)} async-done(((f32[4,2,16,256]{3,2,1,0:T(8,128)}), f32[4,2,16,256]{3,2,1,0:T(8,128)S(1)}, u32[]{:S(2)}, u32[]{:S(2)}) %all-to-all-start.2) | async-done | bytes 131104 | tf_op jit(solution)/shard_map/all_to_all | solution.py:165
  130.9 14.0 %all_gather.11 = bf16[32,2048]{1,0:T(8,128)(2,1)S(1)} all-gather(bf16[32,256]{1,0:T(8,128)(2,1)S(1)} %fusion.25), channel_id=1, replica_groups=mesh['ep'=4,'tp'=8] {'tp'}, dimensions={1}, use_global_device_ids=true | all-gather | bytes 147456 | tf_op jit(solution)/shard_map/all_gather | solution.py:174
  144.9 0.7 copy.93
  (65 shorter events, 5.1 us)
Async XLA Ops:
  7.2 29.7 %copy-start = (bf16[256,2048]{1,0:T(8,128)(2,1)S(1)}, bf16[256,2048]{1,0:T(8,128)(2,1)}, u32[]{:S(2)}) copy-start(bf16[256,2048]{1,0:T(8,128)(2,1)} %param.30) | copy-start | bytes 3145732
  7.2 11.2 %copy-start.3 = (bf16[4,32,256]{2,1,0:T(8,128)(2,1)S(1)}, bf16[4,32,256]{2,1,0:T(8,128)(2,1)}, u32[]{:S(2)}) copy-start(bf16[4,32,256]{2,1,0:T(8,128)(2,1)} %param.23) | copy-start | bytes 196612
  7.2 11.8 %copy-start.2 = (bf16[4,32,2048]{2,1,0:T(8,128)(2,1)S(1)}, bf16[4,32,2048]{2,1,0:T(8,128)(2,1)}, u32[]{:S(2)}) copy-start(bf16[4,32,2048]{2,1,0:T(8,128)(2,1)} %param.21) | copy-start | bytes 1572868
  7.2 58.3 %all-gather.3.cloned.1.call-start = ((), (), s32[]{:S(2)}) async-start(), calls=%async_computation.5 | async-start | bytes 2359296 | tf_op jit(solution)/shard_map/all_gather | solution.py:139
  18.3 6.0 %copy-start.7 = (bf16[4,256]{1,0:T(4,128)(2,1)}, bf16[4,256]{1,0:T(4,128)(2,1)S(1)}, u32[]{:S(2)}) copy-start(bf16[4,256]{1,0:T(4,128)(2,1)S(1)} %get-tuple-element.27) | copy-start | bytes 6148
  21.3 16.7 %copy-start.6 = (bf16[2048]{0:T(1024)(128)(2,1)S(1)}, bf16[2048]{0:T(1024)(128)(2,1)}, u32[]{:S(2)}) copy-start(bf16[2048]{0:T(1024)(128)(2,1)} %param.31) | copy-start | bytes 12292
  21.3 16.7 %copy-start.5 = (s32[32,2]{0,1:T(2,128)S(1)}, s32[32,2]{0,1:T(2,128)}, u32[]{:S(2)}) copy-start(s32[32,2]{0,1:T(2,128)} %param.34) | copy-start | bytes 772
  24.4 42.9 %copy-start.1 = (bf16[32,2048]{1,0:T(8,128)(2,1)S(1)}, bf16[32,2048]{1,0:T(8,128)(2,1)}, u32[]{:S(2)}) copy-start(bf16[32,2048]{1,0:T(8,128)(2,1)} %param.19) | copy-start | bytes 393220
  24.4 43.1 %copy-start.8 = (bf16[2048,4]{0,1:T(4,128)(2,1)S(1)}, bf16[2048,4]{0,1:T(4,128)(2,1)}, u32[]{:S(2)}) copy-start(bf16[2048,4]{0,1:T(4,128)(2,1)} %param.32) | copy-start | bytes 49156
  24.4 43.3 %copy-start.4 = (bf16[2048,8]{0,1:T(8,128)(2,1)S(1)}, bf16[2048,8]{0,1:T(8,128)(2,1)}, u32[]{:S(2)}) copy-start(bf16[2048,8]{0,1:T(8,128)(2,1)} %param.33) | copy-start | bytes 98308
  37.9 82.6 %reduce-scatter.2.cloned.1.call-start = ((), (), s32[]{:S(2)}) async-start(), calls=%async_computation.4 | async-start | bytes 1179648 | tf_op jit(solution)/shard_map/reduce_scatter | solution.py:164
  122.1 8.6 %all-to-all-start.2 = ((f32[4,2,16,256]{3,2,1,0:T(8,128)}), f32[4,2,16,256]{3,2,1,0:T(8,128)S(1)}, u32[]{:S(2)}, u32[]{:S(2)}) async-start(f32[4,2,16,256]{3,2,1,0:T(8,128)} %copy.68), calls=%async_computation.3 | async-start | bytes 262144 | tf_op jit(solution)/shard_map/all_to_all | solution.py:165
Sparse Core Ops, SparseCore 0:
  38.1 27.3 all-gather.2
  89.9 30.5 reduce-scatter.1
